TPU v7x, 32 devices: a whole 2x2x4 slice. The times are simulated.
32 devices in a mesh: sp: 4 (over y, x), dp: 8 (over z, core).
Axes of the slice: x: 2, y: 2, z: 4, core: 2. Of those that a mesh axis runs over, the one named last changes fastest.
Arguments:
- tokens: bfloat16 [8, 1536, 2048], P('dp', 'sp'), may hold values from -6 to 6
- value_act: bfloat16 [8, 1536, 1024], P('dp', 'sp'), may hold values from -6 to 6
- gate_act: bfloat16 [8, 1536, 1024], P('dp', 'sp'), may hold values from -6 to 6
- cotangent: bfloat16 [8, 1536, 1024], P('dp', 'sp'), may hold values from -6 to 6
- value_weight: bfloat16 [2048, 1024], P('dp'), may hold values from -0.1875 to 0.1875
- gate_weight: bfloat16 [2048, 1024], P('dp'), may hold values from -0.1875 to 0.1875
- norm_gain: float32 [1024], replicated, may hold values from 0.1 to 1.9
- norm_bias: float32 [1024], replicated, may hold values from -3 to 3
- mix_weight: bfloat16 [16, 128, 128], replicated, may hold values from -0.5 to 0.5
- mix_bias: float32 [16, 128], replicated, may hold values from 0.1 to 1.9
Outputs:
- tokens_grad: bfloat16 [8, 1536, 2048], P('dp', 'sp')
- value_weight_grad: float32 [2048, 1024], P('dp')
- gate_weight_grad: float32 [2048, 1024], P('dp')
- mix_weight_grad: float32 [16, 128, 128], replicated
- mix_bias_grad: float32 [16, 128], replicated
- norm_gain_grad: float32 [1024], replicated
- norm_bias_grad: float32 [1024], replicated
All inputs are finite; a program needn't handle non-finite values.
Results may differ from a plain program's by a relative error of at most 0.0054.
Values may be sent and summed in bfloat16 or wider, within the bound.
A program may use at most 128 MiB of HBM per device.

v0:
```python
import jax
import jax.numpy as jnp
from jax import lax
from jax.sharding import PartitionSpec as P

EPSILON = 1e-06


def gelu_slope(values):
    cdf_part = 0.5 * (1.0 + lax.erf(values * 0.7071067811865476))
    pdf_part = jnp.exp(-0.5 * values * values) * 0.3989422804014327
    return cdf_part + values * pdf_part


def mixer_backward(value_act, gate_act, cotangent, norm_gain, norm_bias, mix_weight, mix_bias):
    seq_len, channels = value_act.shape
    groups, block_len = (mix_weight.shape[0], mix_weight.shape[1])
    group_dim = channels // groups
    blocks = seq_len // block_len
    value_float = value_act.astype(jnp.float32)
    gate_float = gate_act.astype(jnp.float32)
    activated = jax.nn.gelu(value_float, approximate=False)
    gate_gelu = jax.nn.gelu(gate_float, approximate=False)
    centred = gate_gelu - jnp.mean(gate_gelu, axis=-1, keepdims=True)
    inv_std = lax.rsqrt(jnp.mean(centred * centred, axis=-1, keepdims=True) + EPSILON)
    normed = centred * inv_std
    spread_in = (normed * norm_gain + norm_bias).astype(jnp.bfloat16)
    spread_in = spread_in.reshape(blocks, block_len, groups, group_dim)
    causal = jnp.tril(jnp.ones((block_len, block_len), dtype=bool))
    masked_weight = jnp.where(causal[None], mix_weight, jnp.zeros_like(mix_weight))
    spatial = jnp.einsum(
        "gts,bsgd->btgd", masked_weight, spread_in, preferred_element_type=jnp.float32
    )
    spatial = (spatial + mix_bias.T[None, :, :, None]).reshape(seq_len, channels)
    grad_out = cotangent.astype(jnp.float32)
    grad_act = grad_out * spatial
    grad_spatial = grad_out * activated
    grad_split = grad_spatial.reshape(blocks, block_len, groups, group_dim)
    bias_grad = jnp.sum(grad_split, axis=(0, 3)).T
    spatial_low = grad_split.astype(jnp.bfloat16)
    weight_grad = jnp.einsum(
        "btgd,bsgd->gts", spatial_low, spread_in, preferred_element_type=jnp.float32
    )
    weight_grad = jnp.where(causal[None], weight_grad, jnp.zeros_like(weight_grad))
    grad_norm = jnp.einsum(
        "gts,btgd->bsgd", masked_weight, spatial_low, preferred_element_type=jnp.float32
    )
    grad_norm = grad_norm.reshape(seq_len, channels)
    gain_grad = jnp.sum(grad_norm * normed, axis=0)
    shift_grad = jnp.sum(grad_norm, axis=0)
    grad_hat = grad_norm * norm_gain
    grad_gate = inv_std * (
        grad_hat
        - jnp.mean(grad_hat, axis=-1, keepdims=True)
        - normed * jnp.mean(grad_hat * normed, axis=-1, keepdims=True)
    )
    value_grad = (grad_act * gelu_slope(value_float)).astype(jnp.bfloat16)
    gate_grad = (grad_gate * gelu_slope(gate_float)).astype(jnp.bfloat16)
    return (value_grad, gate_grad, (weight_grad, bias_grad, gain_grad, shift_grad))


def shards(
    tokens,
    value_act,
    gate_act,
    cotangent,
    value_weight,
    gate_weight,
    norm_gain,
    norm_bias,
    mix_weight,
    mix_bias,
):
    value_grad, gate_grad, stats = mixer_backward(
        value_act[0], gate_act[0], cotangent[0], norm_gain, norm_bias, mix_weight, mix_bias
    )
    channels = value_grad.shape[1]
    both_grads = jnp.concatenate((value_grad, gate_grad), axis=1)
    both_weights = jnp.concatenate((value_weight, gate_weight), axis=1)
    input_grad = lax.dot_general(
        both_grads,
        lax.all_gather(both_weights, "dp", axis=0, tiled=True),
        (((1,), (1,)), ((), ())),
        preferred_element_type=jnp.float32,
    ).astype(jnp.bfloat16)
    inputs = tokens[0]
    seq_len, width = inputs.shape
    seq_ways = lax.axis_size("sp")
    data_ways = lax.axis_size("dp")
    part_rows = width // (seq_ways * data_ways)
    reordered = (
        inputs.reshape(seq_len, data_ways, seq_ways, part_rows)
        .transpose(0, 2, 1, 3)
        .reshape(seq_len, width)
    )
    own_terms = lax.psum_scatter(
        lax.dot_general(
            reordered, both_grads, (((0,), (0,)), ((), ())), preferred_element_type=jnp.float32
        ),
        ("sp", "dp"),
        scatter_dimension=0,
        tiled=True,
    )
    weight_sums = lax.all_gather(own_terms, "sp", axis=0, tiled=True)
    totals = lax.psum((stats[0], stats[1], stats[2], stats[3]), ("sp", "dp"))
    return (
        input_grad[None],
        weight_sums[:, :channels],
        weight_sums[:, channels:],
        totals[0],
        totals[1],
        totals[2],
        totals[3],
    )


def solution(mesh):
    placed = (
        P("dp", "sp", None),
        P("dp", "sp", None),
        P("dp", "sp", None),
        P("dp", "sp", None),
        P("dp", None),
        P("dp", None),
        P(),
        P(),
        P(),
        P(),
    )
    return jax.shard_map(
        shards,
        mesh=mesh,
        in_specs=placed,
        out_specs=(P("dp", "sp", None), P("dp", None), P("dp", None), P(), P(), P(), P()),
        check_vma=False,
    )
```

profile of v0, /device:TPU:0, one launch (start us, length us, event | category | flops | bytes accessed | tf_op | source)
XLA Modules:
  0.0 495.3 jit_solution(14789392815174218059)
XLA Ops:
  8.0 0.0 reduce-scatter.4.cloned.1.call-start
  8.1 1.5 copy.42
  9.6 3.5 fusion.95
  13.0 0.0 copy-start.12
  13.0 0.0 copy-start.14
  13.1 1.9 convert_multiply_fusion.1
  15.0 0.1 mul.187
  15.1 0.1 add.56
  15.2 1.2 copy.50
  16.3 1.5 copy.41
  17.8 2.6 copy.59
  20.4 2.7 copy.60
  23.2 0.2 multiply_reduce_fusion.2
  23.4 1.7 reshape.157
  25.1 3.0 convert_multiply_fusion
  28.0 3.6 mul.200
  31.6 3.6 mul.202
  35.2 3.6 mul.177
  38.8 3.6 mul.179
  42.4 5.6 %fusion.92 = (f32[128,16]{0,1:T(8,128)S(1)}, bf16[3,128,16,64]{1,3,0,2:T(8,128)(2,1)S(1)}) fusion(f32[3,128,16,64]{1,0,3,2:T(4,128)} %mul.202, f32[3,128,16,64]{1,0,3,2:T(4,128)} %mul.200, f32[3,128,16,64]{1,0,3,2:T(4,128)} %reshape.157), kind=kLoop, calls=%fused_computation.136 | loop fusion | flops 25163776 | bytes 5513216 | tf_op jit(solution)/shard_map/reduce_sum | solution.py:39
  48.1 4.0 multiply_reduce_fusion
  52.1 1.1 copy-done.1
  53.3 0.5 bitcast_add_fusion
  53.8 1.1 copy.49
  54.9 0.0 copy-done
  54.9 0.8 fusion.77
  55.8 1.1 copy.58
  56.9 1.5 fusion.78
  58.4 8.1 %convolution_bitcast_fusion = f32[2048,2048]{0,1:T(8,128)} fusion(bf16[384,2048]{0,1:T(8,128)(2,1)S(1)} %bitcast.239, bf16[384,1024]{0,1:T(8,128)(2,1)S(1)} %fusion.78, bf16[384,1024]{0,1:T(8,128)(2,1)S(1)} %fusion.77), kind=kOutput, calls=%fused_computation | convolution fusion | flops 3224371200 | bytes 19922944 | tf_op jit(solution)/shard_map/dot_general | solution.py:97
  66.5 17.6 %copy.64 = f32[2048,2048]{1,0:T(8,128)} copy(f32[2048,2048]{0,1:T(8,128)} %convolution_bitcast_fusion) | data formatting | bytes 33554432
  84.1 0.0 reduce-scatter.4.cloned.1.call-update
  84.2 0.0 all-gather.3.cloned.1.call-start
  84.2 1.0 copy-done.11
  85.2 2.1 pad_maximum_fusion.1
  87.3 0.0 all-gather.3.cloned.1.call-update
  87.3 0.0 all-gather.5.cloned.1.call-start
  87.4 253.9 %reduce-scatter.4.cloned.1.call-done = f32[64,2048]{1,0:T(8,128)} async-done(((f32[2048,2048]{1,0:T(8,128)}), f32[64,2048]{1,0:T(8,128)}) %reduce-scatter.4.cloned.1.call-update) | async-done | bytes 524304 | tf_op jit(solution)/shard_map/reduce_scatter | solution.py:96
  341.3 0.0 all-gather.5.cloned.1.call-update
  341.3 0.3 all-reduce.3.cloned.1.call-start
  341.6 2.9 fusion.79
  344.5 0.0 all-reduce.3.cloned.1.call-update
  344.5 0.1 reduce_sum.73
  344.6 0.1 reduce_sum.75
  344.7 37.5 %all-reduce = (f32[16,128]{1,0:T(8,128)}, f32[1024]{0:T(1024)}, f32[1024]{0:T(1024)}) all-reduce(f32[16,128]{1,0:T(8,128)S(1)} %bitcast.240, f32[1024]{0:T(1024)S(1)} %reduce_sum.73, f32[1024]{0:T(1024)S(1)} %reduce_sum.75), channel_id=1, replica_groups=mesh['sp'=4,'dp'=8] {'sp','dp'}, use_global_device_ids=true, to_apply=%region_7.8 | all-reduce | flops 4096 | bytes 32768 | tf_op jit(solution)/shard_map/psum | solution.py:105
  382.1 8.0 %fusion = bf16[1,384,2048]{2,1,0:T(8,128)(2,1)} fusion(bf16[2048,2048]{1,0:T(8,128)(2,1)} %all-gather.3.cloned.1.call-done, bf16[384,1024]{0,1:T(8,128)(2,1)S(1)} %fusion.78, bf16[384,1024]{0,1:T(8,128)(2,1)S(1)} %copy-done.5), kind=kOutput, calls=%fused_computation.2 | convolution fusion | flops 3225157632 | bytes 11534336 | tf_op jit(solution)/shard_map/dot_general | solution.py:80
  390.2 3.1 fusion.97
  393.3 92.3 %all-reduce.3.cloned.1.call-done = f32[16,128,128]{2,1,0:T(8,128)} async-done(((f32[16,128,128]{2,1,0:T(8,128)}), f32[16,128,128]{2,1,0:T(8,128)}) %all-reduce.3.cloned.1.call-update) | async-done | bytes 1048592 | tf_op jit(solution)/shard_map/psum | solution.py:105
  485.5 2.3 copy.85
  (31 shorter events, 0.1 us)
Async XLA Ops:
  8.0 333.3 %reduce-scatter.4.cloned.1.call-start = ((), (), s32[]{:S(2)}) async-start(), calls=%async_computation.4 | async-start | bytes 17301504 | tf_op jit(solution)/shard_map/reduce_scatter | solution.py:96
  13.0 2.0 copy-start.12
  13.0 2.0 copy-start.14
  13.1 2.1 copy-start.9
  42.4 5.6 %copy-start.7 = (f32[3,128,16,64]{1,0,3,2:T(4,128)S(1)}, f32[3,128,16,64]{1,0,3,2:T(4,128)}, u32[]{:S(2)}) copy-start(f32[3,128,16,64]{1,0,3,2:T(4,128)} %mul.177) | copy-start | bytes 4718596
  42.4 5.6 %copy-start.8 = (f32[3,128,16,64]{1,0,3,2:T(4,128)S(1)}, f32[3,128,16,64]{1,0,3,2:T(4,128)}, u32[]{:S(2)}) copy-start(f32[3,128,16,64]{1,0,3,2:T(4,128)} %mul.179) | copy-start | bytes 4718596
  42.4 5.7 %copy-start.10 = (bf16[16,128,128]{2,1,0:T(8,128)(2,1)S(1)}, bf16[16,128,128]{2,1,0:T(8,128)(2,1)}, u32[]{:S(2)}) copy-start(bf16[16,128,128]{2,1,0:T(8,128)(2,1)} %param.18) | copy-start | bytes 1572868
  48.0 4.1 copy-start.6
  48.1 5.2 %copy-start.13 = (f32[16,128]{1,0:T(8,128)S(1)}, f32[16,128]{1,0:T(8,128)}, u32[]{:S(2)}) copy-start(f32[16,128]{1,0:T(8,128)} %param.19) | copy-start | bytes 24580
  52.1 1.1 copy-start.1
  53.8 1.1 copy-start
  55.7 2.7 copy-start.4
  56.9 1.5 copy-start.3
  84.1 1.0 copy-start.11
  84.2 257.4 %copy-start.2 = (f32[3,128,16,64]{1,3,0,2:T(8,128)S(1)}, f32[3,128,16,64]{1,3,0,2:T(8,128)}, u32[]{:S(2)}) copy-start(f32[3,128,16,64]{1,3,0,2:T(8,128)} %copy-done.1) | copy-start | bytes 4718596
  84.2 298.0 %all-gather.3.cloned.1.call-start = ((), (), s32[]{:S(2)}) async-start(), calls=%async_computation.1 | async-start | bytes 9437184 | tf_op jit(solution)/shard_map/all_gather | solution.py:82
  87.3 302.9 %all-gather.5.cloned.1.call-start = ((), (), s32[]{:S(2)}) async-start(), calls=%async_computation.2 | async-start | bytes 2621440 | tf_op jit(solution)/shard_map/all_gather | solution.py:104
  341.3 40.8 %copy-start.5 = (bf16[384,1024]{0,1:T(8,128)(2,1)S(1)}, bf16[384,1024]{0,1:T(8,128)(2,1)}, u32[]{:S(2)}) copy-start(bf16[384,1024]{0,1:T(8,128)(2,1)} %copy-done.4) | copy-start | bytes 2359300
  341.3 144.2 %all-reduce.3.cloned.1.call-start = ((), (), s32[]{:S(2)}) async-start(), calls=%async_computation.3 | async-start | bytes 2097152 | tf_op jit(solution)/shard_map/psum | solution.py:105
Sparse Core Ops, SparseCore 0:
  84.3 256.9 reduce-scatter.3
  347.3 138.1 all-reduce.2
Sparse Core Ops, SparseCore 1:
  87.4 99.9 all-gather.2
  341.4 33.8 all-gather.4
where the time goes:
time: 496 us; the launch traced here: 495 us
  waiting for transfers between devices  346 us (70%)
  local copies, waits for them, and re-layouts  53.1 us (11%)
  blocking collectives  37.5 us (8%)
  matrix products  23.6 us (5%)
  other arithmetic  18.7 us (4%)
  between operations  15.7 us (3%)
    reduce_scatter x1, waiting for transfers between devices, shards(): lax.psum_scatter(lax.dot_general(reordered, both_grads, (((0,), (0,)), ((...  254 us
    psum x1, waiting for transfers between devices, shards(): totals = lax.psum((stats[0], stats[1], stats[2], stats[3]), ('sp', 'dp'))  92.3 us
    psum x1, blocking collectives, shards(): totals = lax.psum((stats[0], stats[1], stats[2], stats[3]), ('sp', 'dp'))  37.5 us
    unnamed x36, local copies, waits for them, and re-layouts  28.8 us
  transfers between devices with their start and end apart: 4, of which 2 were waited for; matrix products, arithmetic and copies ran while one was open for 3% of the time, Pallas kernels for 0%

commit v1 on v0

v1 whole, which is shorter than its diff:
```python
import functools

import jax
import jax.numpy as jnp
from jax import lax
from jax.experimental import pallas as pl
from jax.experimental.pallas import tpu as pltpu
from jax.sharding import PartitionSpec as P

EPSILON = 1e-06
CORES = 2
MESH = pl.DeviceIdType.MESH
F32 = jnp.float32
BF16 = jnp.bfloat16


def remote(src, dst, send, recv, device):
    return pltpu.make_async_remote_copy(
        src_ref=src, dst_ref=dst, send_sem=send, recv_sem=recv, device_id=device, device_id_type=MESH
    )


def position():
    s, d = lax.axis_index("sp"), lax.axis_index("dp")
    return s, d, d // CORES, d % CORES


def greet(ways, levels, s, d, z, c):
    barrier = pltpu.get_barrier_semaphore()
    for k in range(1, ways):
        pl.semaphore_signal(barrier, inc=1, device_id=((s + k) % ways, d), device_id_type=MESH)
    for k in range(1, levels):
        other = ((z + k) % levels) * CORES + c
        pl.semaphore_signal(barrier, inc=1, device_id=(s, other), device_id_type=MESH)
    pl.semaphore_signal(barrier, inc=1, device_id=(s, d + 1 - 2 * c), device_id_type=MESH)
    pl.semaphore_wait(barrier, ways - 1 + levels - 1 + 1)


def phi(values):
    cdf_part = 0.5 * (1.0 + lax.erf(values * 0.7071067811865476))
    pdf_part = jnp.exp(-0.5 * values * values) * 0.3989422804014327
    return cdf_part, cdf_part + values * pdf_part


def mix_kernel(
    ways, levels,
    tokens, weights, value_act, gate_act, cotangent, gain, shift, mix, mix_turned, bias,
    both, pair_tokens, pair_grads, gathered, weight_grad, spatial_sum, gain_grad, shift_grad,
    own_part, swap_part, spread, low, spatial, grad_norm,
    local_sem, core_sem, level_sem, plane_sem, relay_sem,
):
    s, d, z, c = position()
    partner = (s, d + 1 - 2 * c)
    seq_len, channels = value_act.shape
    pairs, double, block_len = mix.shape
    lanes = channels // pairs
    width = weights.shape[1]
    piece = width // ways

    def columns(index):
        return pl.ds(pl.multiple_of(index * piece, piece), piece)

    greet(ways, levels, s, d, z, c)
    level_copies = []
    for k in range(1, levels):
        level_copies.append(remote(
            weights.at[:, columns(s)], gathered.at[z, c, :, columns(s)],
            level_sem.at[0, k - 1], level_sem.at[1, k - 1],
            (s, ((z + k) % levels) * CORES + c),
        ))
    order = sorted(range(levels - 1), key=lambda k: min(k + 1, levels - 1 - k))
    for k in order:
        level_copies[k].start()
    token_swap = remote(tokens, pair_tokens.at[1], core_sem.at[0, 0], core_sem.at[1, 0], partner)
    token_swap.start()
    shard_swap = remote(weights, gathered.at[z, c], core_sem.at[0, 1], core_sem.at[1, 1], partner)
    shard_swap.start()
    token_copy = pltpu.make_async_copy(tokens, pair_tokens.at[0], local_sem.at[0])
    token_copy.start()
    shard_copy = pltpu.make_async_copy(weights, gathered.at[z, c], local_sem.at[1])
    shard_copy.start()

    plane_copies, relays = {}, {}

    def forward(k):
        level_copies[k].wait_recv()
        source = (z + levels - 1 - k) % levels
        block = gathered.at[source, c, :, columns(s)]
        for j in range(1, ways):
            copy = remote(
                block, block, plane_sem.at[0, k, j - 1], plane_sem.at[1, k, j - 1], ((s + j) % ways, d)
            )
            copy.start()
            plane_copies[k, j] = copy
        relay = remote(block, block, relay_sem.at[0, k, 0], relay_sem.at[1, k, 0], partner)
        relay.start()
        relays[k, 0] = relay

    def relay_plane(k, j):
        plane_copies[k, j].wait_recv()
        source = (z + levels - 1 - k) % levels
        block = gathered.at[source, c, :, columns((s + ways - j) % ways)]
        relay = remote(block, block, relay_sem.at[0, k, j], relay_sem.at[1, k, j], partner)
        relay.start()
        relays[k, j] = relay

    weight_grad[...] = jnp.zeros_like(weight_grad)
    spatial_sum[...] = jnp.zeros_like(spatial_sum)
    gain_grad[...] = jnp.zeros_like(gain_grad)
    shift_grad[...] = jnp.zeros_like(shift_grad)
    first_half = lax.broadcasted_iota(jnp.int32, (block_len, lanes), 1) < lanes // 2
    waiting = list(order)
    blocks = seq_len // block_len
    for b in range(blocks):
        rows = pl.ds(b * block_len, block_len)
        gate = gate_act[rows, :].astype(F32)
        gate_cdf, gate_slope = phi(gate)
        gelu = gate * gate_cdf
        centred = gelu - jnp.mean(gelu, axis=-1, keepdims=True)
        inv_std = lax.rsqrt(jnp.mean(centred * centred, axis=-1, keepdims=True) + EPSILON)
        normed = centred * inv_std
        spread[...] = (normed * gain[...] + shift[...]).astype(BF16)
        value = value_act[rows, :].astype(F32)
        value_cdf, value_slope = phi(value)
        grad_out = cotangent[rows, :].astype(F32)
        grad_spatial = grad_out * (value * value_cdf)
        spatial_sum[...] += grad_spatial
        low[...] = grad_spatial.astype(BF16)
        for p in range(pairs):
            cut = pl.ds(p * lanes, lanes)
            inner = spread[:, cut]
            mixed = jnp.dot(mix[p], inner, preferred_element_type=F32)
            spatial[:, cut] = jnp.where(first_half, mixed[:block_len], mixed[block_len:]) + bias[:, cut]
            piece_low = low[:, cut]
            zero = jnp.zeros_like(piece_low)
            apart = jnp.concatenate(
                (jnp.where(first_half, piece_low, zero), jnp.where(first_half, zero, piece_low)), axis=0
            )
            weight_grad[p] += lax.dot_general(
                apart, inner, (((1,), (1,)), ((), ())), preferred_element_type=F32
            )
            grad_norm[:, cut] = jnp.dot(mix_turned[p], apart, preferred_element_type=F32)
        back = grad_norm[...]
        gain_grad[...] += jnp.sum(back * normed, axis=0, keepdims=True)
        shift_grad[...] += jnp.sum(back, axis=0, keepdims=True)
        hat = back * gain[...]
        grad_gate = inv_std * (
            hat
            - jnp.mean(hat, axis=-1, keepdims=True)
            - normed * jnp.mean(hat * normed, axis=-1, keepdims=True)
        )
        value_grad = (grad_out * spatial[...] * value_slope).astype(BF16)
        gate_grad = (grad_gate * gate_slope).astype(BF16)
        both[rows, :channels] = value_grad
        both[rows, channels:] = gate_grad
        chosen = jnp.full(value_grad.shape, c, jnp.int32) == 0
        own_part[rows, :] = jnp.where(chosen, value_grad.astype(F32), gate_grad.astype(F32)).astype(BF16)
        swap_part[rows, :] = jnp.where(chosen, gate_grad.astype(F32), value_grad.astype(F32)).astype(BF16)
        if waiting and b < blocks - 1:
            forward(waiting.pop(0))
    grad_copy = pltpu.make_async_copy(own_part, pair_grads.at[0], local_sem.at[2])
    grad_copy.start()
    grad_swap = remote(swap_part, pair_grads.at[1], core_sem.at[0, 2], core_sem.at[1, 2], partner)
    grad_swap.start()
    while waiting:
        forward(waiting.pop(0))
    for k in order:
        for j in range(1, ways):
            relay_plane(k, j)
    token_copy.wait()
    shard_copy.wait()
    grad_copy.wait()
    for copy in level_copies:
        copy.wait_send()
    for key in plane_copies:
        plane_copies[key].wait_send()
    for copy in (token_swap, shard_swap, grad_swap):
        copy.wait()
    for key in relays:
        relays[key].wait()


def sum_kernel(
    ways, levels,
    part, mix_part, small,
    summed, mix_out, small_out,
    plane_in, level_out, level_in, own_sum, final, final_in,
    mix_in, mix_low, mix_plane, mix_sum, mix_level_out, mix_level, small_in, small_plane, small_level,
    core_sem, plane_sem, level_sem, gather_sem, mix_sem, mix_level_sem, mix_up_sem, mix_out_sem,
    small_sem, small_level_sem,
):
    s, d, z, c = position()
    partner = (s, d + 1 - 2 * c)
    half = part.shape[-1]

    def in_plane(k):
        return ((s + k) % ways, d)

    def in_level(k):
        return (s, ((z + k) % levels) * CORES + c)

    greet(ways, levels, s, d, z, c)
    mix_swap = remote(mix_part.at[1 - c], mix_in, core_sem.at[0, 0], core_sem.at[1, 0], partner)
    mix_swap.start()
    small_swap = remote(small, small_in, core_sem.at[0, 1], core_sem.at[1, 1], partner)
    small_swap.start()
    copies = {}

    def send_chunk(i):
        target = (z + 1 + i) % levels
        for k in range(1, ways):
            copy = remote(
                part.at[target, :, (s + k) % ways], plane_in.at[i, k - 1],
                plane_sem.at[0, i, k - 1], plane_sem.at[1, i, k - 1], in_plane(k),
            )
            copy.start()
            copies[i, k] = copy

    pending = []

    send_chunk(0)
    mix_swap.wait()
    small_swap.wait()
    mix_low[...] = (mix_part[c] + mix_in[...]).astype(BF16)
    small_plane[s] = small[...] + small_in[...]
    mix_copies, small_copies = [], []
    for k in range(1, ways):
        mix_copies.append(remote(
            mix_low.at[(s + k) % ways], mix_plane.at[k - 1],
            mix_sem.at[0, k - 1], mix_sem.at[1, k - 1], in_plane(k),
        ))
        small_copies.append(remote(
            small_plane.at[s], small_plane.at[s],
            small_sem.at[0, k - 1], small_sem.at[1, k - 1], in_plane(k),
        ))
    for copy in mix_copies + small_copies:
        copy.start()
    for i in range(1, levels):
        send_chunk(i)

    mix_level_copies, small_level_copies, mix_up, mix_gather = [], [], [], []

    def mix_stage(stage):
        if stage == 0:
            for copy in mix_copies + small_copies:
                copy.wait()
            total = mix_low[s].astype(F32)
            for k in range(1, ways):
                total = total + mix_plane[k - 1].astype(F32)
            mix_sum[...] = total
            mix_level_out[...] = total.astype(BF16)
            gathered = small_plane[0]
            for k in range(1, ways):
                gathered = gathered + small_plane[k]
            small_level[z] = gathered
            for k in range(1, levels):
                mix_level_copies.append(remote(
                    mix_level_out.at[(z + k) % levels], mix_level.at[k - 1],
                    mix_level_sem.at[0, k - 1], mix_level_sem.at[1, k - 1], in_level(k),
                ))
                small_level_copies.append(remote(
                    small_level.at[z], small_level.at[z],
                    small_level_sem.at[0, k - 1], small_level_sem.at[1, k - 1], in_level(k),
                ))
            for copy in mix_level_copies + small_level_copies:
                copy.start()
        elif stage == 1:
            for copy in mix_level_copies + small_level_copies:
                copy.wait()
            total = mix_sum[z]
            for k in range(1, levels):
                total = total + mix_level[k - 1].astype(F32)
            mix_out[c, s, z] = total.astype(BF16)
            gathered = small_level[0]
            for k in range(1, levels):
                gathered = gathered + small_level[k]
            small_out[...] = gathered
            for k in range(1, levels):
                block = mix_out.at[c, s, z]
                mix_up.append(remote(
                    block, block, mix_up_sem.at[0, k - 1], mix_up_sem.at[1, k - 1], in_level(k)
                ))
                mix_up[-1].start()
        else:
            for copy in mix_up:
                copy.wait()
            for k in range(1, ways):
                block = mix_out.at[c, s]
                mix_gather.append(remote(
                    block, block, mix_out_sem.at[0, k - 1], mix_out_sem.at[1, k - 1], in_plane(k)
                ))
                mix_gather[-1].start()

    stages = [0, 1, 2]
    level_copies = []
    for i in range(levels):
        target = (z + 1 + i) % levels
        total = part[target, :, s].astype(F32)
        for k in range(1, ways):
            copies[i, k].wait_recv()
            total = total + plane_in[i, k - 1].astype(F32)
        if i < levels - 1:
            level_out[i] = total.astype(BF16)
            copy = remote(
                level_out.at[i], level_in.at[i], level_sem.at[0, i], level_sem.at[1, i], in_level(i + 1)
            )
            copy.start()
            level_copies.append(copy)
            if stages:
                mix_stage(stages.pop(0))
        else:
            own_sum[...] = total
    total = own_sum[...]
    for i in range(levels - 1):
        level_copies[i].wait_recv()
        total = total + level_in[i].astype(F32)
    final[...] = total
    final_swap = remote(final.at[1 - c], final_in, core_sem.at[0, 2], core_sem.at[1, 2], partner)
    final_swap.start()
    while stages:
        mix_stage(stages.pop(0))
    final_swap.wait()
    mine, theirs = final[c], final_in[...]
    lower = jnp.full(mine.shape, c, jnp.int32) == 0
    summed[s, :, :half] = jnp.where(lower, mine, theirs).astype(BF16)
    summed[s, :, half:] = jnp.where(lower, theirs, mine).astype(BF16)
    gather = []
    for k in range(1, ways):
        copy = remote(
            summed.at[s], summed.at[s], gather_sem.at[0, k - 1], gather_sem.at[1, k - 1], in_plane(k)
        )
        copy.start()
        gather.append(copy)
    for copy in mix_gather:
        copy.wait()
    mix_back = remote(mix_out.at[c], mix_out.at[c], core_sem.at[0, 3], core_sem.at[1, 3], partner)
    mix_back.start()
    mix_back.wait()
    for copy in gather:
        copy.wait()
    for copy in level_copies:
        copy.wait_send()
    for key in copies:
        copies[key].wait_send()


def shards(
    tokens,
    value_act,
    gate_act,
    cotangent,
    value_weight,
    gate_weight,
    norm_gain,
    norm_bias,
    mix_weight,
    mix_bias,
):
    ways = lax.axis_size("sp")
    levels = lax.axis_size("dp") // CORES
    inputs = tokens[0]
    seq_len, width = inputs.shape
    channels = value_act.shape[2]
    groups, block_len = mix_weight.shape[0], mix_weight.shape[1]
    group_dim = channels // groups
    pairs = groups // 2
    rows = value_weight.shape[0]
    vmem = pl.BlockSpec(memory_space=pltpu.VMEM)
    hbm = pl.BlockSpec(memory_space=pl.ANY)
    sems = pltpu.SemaphoreType.DMA
    weights = jnp.concatenate((value_weight, gate_weight), axis=1)
    causal = jnp.tril(jnp.ones((block_len, block_len), dtype=bool))
    masked = jnp.where(causal[None], mix_weight, jnp.zeros_like(mix_weight))
    mix = masked.reshape(pairs, 2 * block_len, block_len)
    bias = jnp.repeat(mix_bias.T, group_dim, axis=1)
    shape = jax.ShapeDtypeStruct
    both, pair_tokens, pair_grads, gathered, weight_grad, spatial_sum, gain_grad, shift_grad = pl.pallas_call(
        functools.partial(mix_kernel, ways, levels),
        out_shape=(
            shape((seq_len, 2 * channels), BF16),
            shape((CORES, seq_len, width), BF16),
            shape((CORES, seq_len, channels), BF16),
            shape((levels, CORES, rows, 2 * channels), BF16),
            shape((pairs, 2 * block_len, block_len), F32),
            shape((block_len, channels), F32),
            shape((1, channels), F32),
            shape((1, channels), F32),
        ),
        in_specs=[vmem] * 10,
        out_specs=(vmem, hbm, hbm, hbm, vmem, vmem, vmem, vmem),
        scratch_shapes=[
            pltpu.VMEM((seq_len, channels), BF16),
            pltpu.VMEM((seq_len, channels), BF16),
            pltpu.VMEM((block_len, channels), BF16),
            pltpu.VMEM((block_len, channels), BF16),
            pltpu.VMEM((block_len, channels), F32),
            pltpu.VMEM((block_len, channels), F32),
            sems((3,)),
            sems((2, 3)),
            sems((2, levels - 1)),
            sems((2, levels - 1, ways - 1)),
            sems((2, levels - 1, ways)),
        ],
        compiler_params=pltpu.CompilerParams(
            collective_id=0, has_side_effects=True, vmem_limit_bytes=40 * 1024 * 1024
        ),
        name="mix",
    )(
        inputs, weights, value_act[0], gate_act[0], cotangent[0],
        norm_gain[None], norm_bias[None], mix, mix.transpose(0, 2, 1), bias,
    )
    part = lax.dot_general(
        pair_tokens.reshape(CORES * seq_len, width),
        pair_grads.reshape(CORES * seq_len, channels),
        (((0,), (0,)), ((), ())),
        preferred_element_type=F32,
    ).astype(BF16)
    share = rows // ways
    part = part.reshape(levels, CORES, ways, share, channels)
    low_rows = groups * block_len // (CORES * ways * levels)
    mix_part = weight_grad.reshape(CORES, ways, levels, low_rows, block_len)
    bias_grad = jnp.sum(spatial_sum.reshape(block_len, groups, group_dim), axis=-1).T
    lanes = 128
    small = jnp.concatenate((bias_grad.reshape(-1), gain_grad[0], shift_grad[0])).reshape(-1, lanes)
    input_grad = lax.dot_general(
        both, gathered.reshape(width, 2 * channels), (((1,), (1,)), ((), ())), preferred_element_type=F32
    ).astype(BF16)
    summed, mix_out, small_out = pl.pallas_call(
        functools.partial(sum_kernel, ways, levels),
        out_shape=(
            shape((ways, share, 2 * channels), BF16),
            shape(mix_part.shape, BF16),
            shape(small.shape, F32),
        ),
        in_specs=[vmem] * 3,
        out_specs=(vmem,) * 3,
        scratch_shapes=[
            pltpu.VMEM((levels, ways - 1, CORES, share, channels), BF16),
            pltpu.VMEM((levels - 1, CORES, share, channels), BF16),
            pltpu.VMEM((levels - 1, CORES, share, channels), BF16),
            pltpu.VMEM((CORES, share, channels), F32),
            pltpu.VMEM((CORES, share, channels), F32),
            pltpu.VMEM((share, channels), F32),
            pltpu.VMEM(mix_part.shape[1:], F32),
            pltpu.VMEM(mix_part.shape[1:], BF16),
            pltpu.VMEM((ways - 1,) + mix_part.shape[2:], BF16),
            pltpu.VMEM(mix_part.shape[2:], F32),
            pltpu.VMEM(mix_part.shape[2:], BF16),
            pltpu.VMEM((levels - 1,) + mix_part.shape[3:], BF16),
            pltpu.VMEM(small.shape, F32),
            pltpu.VMEM((ways,) + small.shape, F32),
            pltpu.VMEM((levels,) + small.shape, F32),
            sems((2, 4)),
            sems((2, levels, ways - 1)),
            sems((2, levels - 1)),
            sems((2, ways - 1)),
            sems((2, ways - 1)),
            sems((2, levels - 1)),
            sems((2, levels - 1)),
            sems((2, ways - 1)),
            sems((2, ways - 1)),
            sems((2, levels - 1)),
        ],
        compiler_params=pltpu.CompilerParams(
            collective_id=1, has_side_effects=True, vmem_limit_bytes=48 * 1024 * 1024
        ),
        name="sum",
    )(part, mix_part, small)
    weight_sums = summed.reshape(rows, 2 * channels).astype(F32)
    mix_grad = jnp.where(causal[None], mix_out.reshape(groups, block_len, block_len).astype(F32), 0.0)
    small_out = small_out.reshape(-1)
    biases = groups * block_len
    return (
        input_grad[None],
        weight_sums[:, :channels],
        weight_sums[:, channels:],
        mix_grad,
        small_out[:biases].reshape(groups, block_len),
        small_out[biases:biases + channels],
        small_out[biases + channels:],
    )


def solution(mesh):
    placed = (
        P("dp", "sp", None),
        P("dp", "sp", None),
        P("dp", "sp", None),
        P("dp", "sp", None),
        P("dp", None),
        P("dp", None),
        P(),
        P(),
        P(),
        P(),
    )
    return jax.shard_map(
        shards,
        mesh=mesh,
        in_specs=placed,
        out_specs=(P("dp", "sp", None), P("dp", None), P("dp", None), P(), P(), P(), P()),
        check_vma=False,
    )
```

time: 496 us -> 155 us (0.31)
  waiting for transfers between devices: 346 us -> 0 us
  Pallas kernels: 0 us -> 122 us
  local copies, waits for them, and re-layouts: 53.1 us -> 11.2 us
  blocking collectives: 37.5 us -> 0 us
  between operations: 15.7 us -> 0.83 us
  other arithmetic: 18.7 us -> 3.93 us
  matrix products: 23.6 us -> 17.3 us
    reduce_scatter x1 -> x0, waiting for transfers between devices: 254 us -> none  [shards(): lax.psum_scatter(lax.dot_general(reordered, both_grads, (((0,), (0,)), ((...]
    pallas_call x0 -> x2, Pallas kernels: none -> 122 us  [the longest x1 71.3 us: shards(): pl.pallas_call(functools.partial(sum_kernel, ways, levels), out_shape=(sh...]
    psum x1 -> x0, waiting for transfers between devices: 92.3 us -> none  [shards(): totals = lax.psum((stats[0], stats[1], stats[2], stats[3]), ('sp', 'dp'))]
    psum x1 -> x0, blocking collectives: 37.5 us -> none  [shards(): totals = lax.psum((stats[0], stats[1], stats[2], stats[3]), ('sp', 'dp'))]
    unnamed x36 -> x28, local copies, waits for them, and re-layouts: 28.8 us -> 6.1 us
    mul x5 -> x0, local copies, waits for them, and re-layouts: 14.4 us -> none  [the longest x2 7.2 us: mixer_backward(): gate_gelu = jax.nn.gelu(gate_float, approximate=False)]
    reduce_sum x3 -> x1, other arithmetic: 9.31 us -> 0.04 us  [shards(): jnp.sum(spatial_sum.reshape(block_len, groups, group_dim), axis=-1)]
    dot_general x5 -> x2, matrix products: 23.6 us -> 17.3 us  [the longest x1 10.2 us: shards(): lax.dot_general(both, gathered.reshape(width, 2 * channels), (((1,), (1,)...]
  transfers between devices with their start and end apart: 4 -> 0, of which waited for: 2 -> 0; matrix products, arithmetic and copies ran while one was open for 3% -> 0% of each run, Pallas kernels for 0% -> 0%
where the time goes in v1:
time: 155 us
  Pallas kernels  122 us (79%)
  matrix products  17.3 us (11%)
  local copies, waits for them, and re-layouts  11.2 us (7%)
  other arithmetic  3.93 us (3%)
    pallas_call x1, Pallas kernels, shards(): pl.pallas_call(functools.partial(sum_kernel, ways, levels), out_shape=(sh...  71.3 us
    pallas_call x1, Pallas kernels, shards(): pl.pallas_call(functools.partial(mix_kernel, ways, levels), out_shape=(sh...  50.6 us
    dot_general x1, matrix products, shards(): lax.dot_general(both, gathered.reshape(width, 2 * channels), (((1,), (1,)...  10.2 us
    dot_general x1, matrix products, shards(): lax.dot_general(pair_tokens.reshape(CORES * seq_len, width), pair_grads.r...  7.1 us
    unnamed x28, local copies, waits for them, and re-layouts  6.1 us

profile of v1, /device:TPU:0, one launch (start us, length us, event | category | flops | bytes accessed | tf_op | source)
XLA Modules:
  0.0 155.2 jit_solution(4407245810866317412)
XLA Ops:
  0.6 0.0 copy-start.13
  0.7 1.1 broadcast_select_fusion
  1.7 0.2 copy.20
  2.0 0.0 copy-start
  2.0 0.0 copy-start.8
  2.0 0.0 copy-start.9
  2.0 0.0 copy-done.13
  2.0 0.8 broadcast_in_dim.44
  2.9 1.2 copy.21.bias
  4.1 0.0 copy-start.3
  4.1 0.0 copy-start.4
  4.1 1.4 pad_maximum_fusion.weights
  5.5 0.0 copy-done
  5.5 0.0 copy-done.8
  5.6 0.0 copy-done.9
  5.6 0.0 copy-done.3
  5.6 0.2 copy-done.4
  5.8 0.0 copy-start.5
  5.8 1.1 copy-done.5
  6.9 50.6 %mix.1 = (bf16[384,2048]{1,0:T(8,128)(2,1)S(1)}, bf16[2,384,2048]{2,1,0:T(8,128)(2,1)S(1)}, bf16[2,384,1024]{2,1,0:T(8,128)(2,1)S(1)}, bf16[4,2,256,2048]{3,2,1,...) custom-call(bf16[384,2048]{1,0:T(8,128)(2,1)S(1)} %bitcast.42, ...), custom_call_target="tpu_custom_call" | custom-call | tf_op jit(solution)/shard_map/mix/pallas_call | solution.py:377
  57.5 0.0 copy-start.1
  57.5 1.0 copy-done.1
  58.5 0.0 copy-start.6
  58.5 0.8 copy-done.6
  59.3 0.0 copy-start.10
  59.3 1.7 %copy-done.10 = bf16[2,384,2048]{2,1,0:T(8,128)(2,1)} copy-done((bf16[2,384,2048]{2,1,0:T(8,128)(2,1)}, bf16[2,384,2048]{2,1,0:T(8,128)(2,1)S(1)}, u32[]{:S(2)}) %copy-start.10) | copy-done | bytes 3145752
  61.0 0.0 copy-start.11
  61.0 1.2 copy-done.11
  62.2 0.0 copy-start.7
  62.2 0.0 copy-start.12
  62.2 10.2 %fusion = bf16[1,384,2048]{2,1,0:T(8,128)(2,1)} fusion(bf16[384,2048]{1,0:T(8,128)(2,1)S(1)} %get-tuple-element.18, bf16[2048,2048]{1,0:T(8,128)(2,1)} %bitcast.56), kind=kOutput, calls=%fused_computation.2 | convolution fusion | flops 3222011904 | bytes 11534336 | tf_op jit(solution)/shard_map/dot_general | solution.py:425
  72.5 0.0 copy-done.7
  72.5 0.2 copy.23
  72.7 0.0 copy-done.12
  72.7 0.0 copy-start.2
  72.8 7.1 %bitcast_convert_fusion = bf16[2048,1024]{1,0:T(8,128)(2,1)} fusion(bf16[2,384,2048]{2,1,0:T(8,128)(2,1)} %copy-done.10, bf16[2,384,1024]{2,1,0:T(8,128)(2,1)S(1)} %copy-done.12), kind=kOutput, calls=%fused_computation | convolution fusion | flops 3223322624 | bytes 8912896 | tf_op jit(solution)/shard_map/dot_general | solution.py:412
  79.8 0.0 copy-done.2
  79.8 71.3 %sum.1 = (bf16[4,64,2048]{2,1,0:T(8,128)(2,1)S(1)}, bf16[2,4,4,64,128]{4,3,2,1,0:T(8,128)(2,1)S(1)}, f32[32,128]{1,0:T(8,128)S(1)}) custom-call(bf16[4,2,4,64,1024]{4,3,2,1,0:T(8,128)(2,1)} %bitcast.52, f32[2,4,4,64,128]{4,3,2,1,0:T(8,128)S(1)} %bitcast.43, f32[32,128]{1,0:T(8,128)S(1)} %maximum_bitcast_fusion.small), custom_call_target="tpu_custom_call" | custom-call | tf_op jit(solution)/shard_map/sum/pallas_call | solution.py:428
  151.2 0.6 slice.24
  151.8 0.6 slice_bitcast_fusion
  152.4 1.1 convert_select_fusion
  153.4 0.3 bitcast_convert_fusion.1
  153.8 1.5 fusion.1
  (3 shorter events, 0.1 us)
Async XLA Ops:
  0.6 1.4 copy-start.13
  2.0 3.6 %copy-start = (bf16[1,384,2048]{2,1,0:T(8,128)(2,1)S(1)}, bf16[1,384,2048]{2,1,0:T(8,128)(2,1)}, u32[]{:S(2)}) copy-start(bf16[1,384,2048]{2,1,0:T(8,128)(2,1)} %param.10) | copy-start | bytes 4718596
  2.0 3.6 %copy-start.8 = (f32[1024]{0:T(1024)S(1)}, f32[1024]{0:T(1024)}, u32[]{:S(2)}) copy-start(f32[1024]{0:T(1024)} %param.16) | copy-start | bytes 12292
  2.0 3.6 %copy-start.9 = (f32[1024]{0:T(1024)S(1)}, f32[1024]{0:T(1024)}, u32[]{:S(2)}) copy-start(f32[1024]{0:T(1024)} %param.17) | copy-start | bytes 12292
  4.1 1.5 copy-start.3
  4.1 1.7 %copy-start.4 = (bf16[1,384,1024]{2,1,0:T(8,128)(2,1)S(1)}, bf16[1,384,1024]{2,1,0:T(8,128)(2,1)}, u32[]{:S(2)}) copy-start(bf16[1,384,1024]{2,1,0:T(8,128)(2,1)} %param.12) | copy-start | bytes 2359300
  5.8 1.1 copy-start.5
  57.5 1.0 copy-start.1
  58.5 0.8 copy-start.6
  59.3 1.7 %copy-start.10 = (bf16[2,384,2048]{2,1,0:T(8,128)(2,1)}, bf16[2,384,2048]{2,1,0:T(8,128)(2,1)S(1)}, u32[]{:S(2)}) copy-start(bf16[2,384,2048]{2,1,0:T(8,128)(2,1)S(1)} %get-tuple-element.20) | copy-start | bytes 9437188
  61.0 1.2 copy-start.11
  62.2 10.2 %copy-start.7 = (f32[128,1024]{1,0:T(8,128)S(1)}, f32[128,1024]{1,0:T(8,128)}, u32[]{:S(2)}) copy-start(f32[128,1024]{1,0:T(8,128)} %copy-done.6) | copy-start | bytes 1572868
  62.2 10.5 %copy-start.12 = (bf16[2,384,1024]{2,1,0:T(8,128)(2,1)S(1)}, bf16[2,384,1024]{2,1,0:T(8,128)(2,1)}, u32[]{:S(2)}) copy-start(bf16[2,384,1024]{2,1,0:T(8,128)(2,1)} %copy-done.11) | copy-start | bytes 4718596
  72.7 7.1 %copy-start.2 = (f32[8,256,128]{2,1,0:T(8,128)S(1)}, f32[8,256,128]{2,1,0:T(8,128)}, u32[]{:S(2)}) copy-start(f32[8,256,128]{2,1,0:T(8,128)} %copy-done.1) | copy-start | bytes 3145732

commit v2 on v1

v2 whole, which is shorter than its diff:
```python
import functools

import jax
import jax.numpy as jnp
from jax import lax
from jax.experimental import pallas as pl
from jax.experimental.pallas import tpu as pltpu
from jax.sharding import PartitionSpec as P

EPSILON = 1e-06
CORES = 2
MESH = pl.DeviceIdType.MESH
F32 = jnp.float32
BF16 = jnp.bfloat16


def remote(src, dst, send, recv, device):
    return pltpu.make_async_remote_copy(
        src_ref=src, dst_ref=dst, send_sem=send, recv_sem=recv, device_id=device, device_id_type=MESH
    )


def position():
    s, d = lax.axis_index("sp"), lax.axis_index("dp")
    return s, d, d // CORES, d % CORES


def greet(ways, levels, s, d, z, c):
    barrier = pltpu.get_barrier_semaphore()
    for k in range(1, ways):
        pl.semaphore_signal(barrier, inc=1, device_id=((s + k) % ways, d), device_id_type=MESH)
    for k in range(1, levels):
        other = ((z + k) % levels) * CORES + c
        pl.semaphore_signal(barrier, inc=1, device_id=(s, other), device_id_type=MESH)
    pl.semaphore_signal(barrier, inc=1, device_id=(s, d + 1 - 2 * c), device_id_type=MESH)
    pl.semaphore_wait(barrier, ways - 1 + levels - 1 + 1)


def phi(values):
    cdf_part = 0.5 * (1.0 + lax.erf(values * 0.7071067811865476))
    pdf_part = jnp.exp(-0.5 * values * values) * 0.3989422804014327
    return cdf_part, cdf_part + values * pdf_part


def kernel(
    ways, levels,
    tokens, weights, value_act, gate_act, cotangent, gain, shift, mix, mix_turned, bias,
    input_grad, summed, mix_out, small_out,
    both, peer_tokens, peer_grads, gathered, weight_grad, spatial_sum, gain_grad, shift_grad,
    own_part, swap_part, spread, low, spatial, grad_norm,
    part, mix_part, small,
    plane_in, level_out, level_in, own_sum, final, final_in,
    mix_in, mix_low, mix_plane, mix_sum, mix_level_out, mix_level, small_in, small_plane, small_level,
    pair_sem, shard_sem, spread_sem, relay_sem,
    core_sem, plane_sem, level_sem, gather_sem, mix_sem, mix_level_sem, mix_up_sem, mix_out_sem,
    small_sem, small_level_sem,
):
    s, d, z, c = position()
    partner = (s, d + 1 - 2 * c)
    seq_len, channels = value_act.shape
    pairs, double, block_len = mix.shape
    lanes = channels // pairs
    groups = 2 * pairs
    rows_own, width = weights.shape
    piece = width // ways
    model = tokens.shape[1]
    depth = model // levels

    def columns(index):
        return pl.ds(pl.multiple_of(index * piece, piece), piece)

    def in_plane(k):
        return ((s + k) % ways, d)

    def in_level(k):
        return (s, ((z + k) % levels) * CORES + c)

    greet(ways, levels, s, d, z, c)
    shard_copies = []
    for k in range(1, levels):
        shard_copies.append(remote(
            weights.at[:, columns(s)], gathered.at[z, c, :, columns(s)],
            shard_sem.at[0, k - 1], shard_sem.at[1, k - 1], in_level(k),
        ))
    order = sorted(range(levels - 1), key=lambda k: min(k + 1, levels - 1 - k))
    for k in order:
        shard_copies[k].start()
    token_swap = remote(tokens, peer_tokens, pair_sem.at[0, 0], pair_sem.at[1, 0], partner)
    token_swap.start()
    shard_swap = remote(weights, gathered.at[z, c], pair_sem.at[0, 1], pair_sem.at[1, 1], partner)
    shard_swap.start()

    spreads, relays = {}, {}

    def level_of(k):
        return (z + levels - 1 - k) % levels

    def forward(k):
        shard_copies[k].wait_recv()
        block = gathered.at[level_of(k), c, :, columns(s)]
        for j in range(1, ways):
            copy = remote(
                block, block, spread_sem.at[0, k, j - 1], spread_sem.at[1, k, j - 1], in_plane(j)
            )
            copy.start()
            spreads[k, j] = copy
        relay = remote(block, block, relay_sem.at[0, k, 0], relay_sem.at[1, k, 0], partner)
        relay.start()
        relays[k, 0] = relay

    def relay_all(k):
        for j in range(1, ways):
            spreads[k, j].wait_recv()
            block = gathered.at[level_of(k), c, :, columns((s + ways - j) % ways)]
            relay = remote(block, block, relay_sem.at[0, k, j], relay_sem.at[1, k, j], partner)
            relay.start()
            relays[k, j] = relay

    def project(shard, index):
        cut = pl.ds(pl.multiple_of(index * rows_own, rows_own), rows_own)
        input_grad[:, cut] = lax.dot_general(
            both[...], shard, (((1,), (1,)), ((), ())), preferred_element_type=F32
        ).astype(BF16)

    def project_level(k):
        level = level_of(k)
        for j in range(ways):
            relays[k, j].wait_recv()
        for core in range(CORES):
            project(gathered[level, core], level * CORES + core)

    weight_grad[...] = jnp.zeros_like(weight_grad)
    spatial_sum[...] = jnp.zeros_like(spatial_sum)
    gain_grad[...] = jnp.zeros_like(gain_grad)
    shift_grad[...] = jnp.zeros_like(shift_grad)
    lane = lax.broadcasted_iota(jnp.int32, (block_len, lanes), 1)
    first_half = lane < lanes // 2
    blocks = seq_len // block_len
    early, late = order[:blocks - 1], order[blocks - 1:]
    for b in range(blocks):
        rows = pl.ds(b * block_len, block_len)
        gate = gate_act[rows, :].astype(F32)
        gate_cdf, gate_slope = phi(gate)
        gelu = gate * gate_cdf
        centred = gelu - jnp.mean(gelu, axis=-1, keepdims=True)
        inv_std = lax.rsqrt(jnp.mean(centred * centred, axis=-1, keepdims=True) + EPSILON)
        normed = centred * inv_std
        spread[...] = (normed * gain[...] + shift[...]).astype(BF16)
        value = value_act[rows, :].astype(F32)
        value_cdf, value_slope = phi(value)
        grad_out = cotangent[rows, :].astype(F32)
        grad_spatial = grad_out * (value * value_cdf)
        spatial_sum[...] += grad_spatial
        low[...] = grad_spatial.astype(BF16)
        for p in range(pairs):
            cut = pl.ds(p * lanes, lanes)
            inner = spread[:, cut]
            mixed = jnp.dot(mix[p], inner, preferred_element_type=F32)
            spatial[:, cut] = jnp.where(first_half, mixed[:block_len], mixed[block_len:]) + bias[:, cut]
            piece_low = low[:, cut]
            zero = jnp.zeros_like(piece_low)
            apart = jnp.concatenate(
                (jnp.where(first_half, piece_low, zero), jnp.where(first_half, zero, piece_low)), axis=0
            )
            weight_grad[p] += lax.dot_general(
                apart, inner, (((1,), (1,)), ((), ())), preferred_element_type=F32
            )
            grad_norm[:, cut] = jnp.dot(mix_turned[p], apart, preferred_element_type=F32)
        back = grad_norm[...]
        gain_grad[...] += jnp.sum(back * normed, axis=0, keepdims=True)
        shift_grad[...] += jnp.sum(back, axis=0, keepdims=True)
        hat = back * gain[...]
        grad_gate = inv_std * (
            hat
            - jnp.mean(hat, axis=-1, keepdims=True)
            - normed * jnp.mean(hat * normed, axis=-1, keepdims=True)
        )
        value_grad = (grad_out * spatial[...] * value_slope).astype(BF16)
        gate_grad = (grad_gate * gate_slope).astype(BF16)
        both[rows, :channels] = value_grad
        both[rows, channels:] = gate_grad
        chosen = jnp.full(value_grad.shape, c, jnp.int32) == 0
        own_part[rows, :] = jnp.where(chosen, value_grad.astype(F32), gate_grad.astype(F32)).astype(BF16)
        swap_part[rows, :] = jnp.where(chosen, gate_grad.astype(F32), value_grad.astype(F32)).astype(BF16)
        if b < len(early):
            forward(early[b])
    grad_swap = remote(swap_part, peer_grads, pair_sem.at[0, 2], pair_sem.at[1, 2], partner)
    grad_swap.start()

    mix_part[...] = weight_grad[...].reshape(mix_part.shape)
    mix_swap = remote(mix_part.at[1 - c], mix_in, core_sem.at[0, 0], core_sem.at[1, 0], partner)
    mix_swap.start()
    sums = jnp.zeros((block_len, lanes), F32)
    for p in range(pairs):
        terms = spatial_sum[:, pl.ds(p * lanes, lanes)]
        lower = jnp.sum(jnp.where(first_half, terms, 0.0), axis=1, keepdims=True)
        upper = jnp.sum(jnp.where(first_half, 0.0, terms), axis=1, keepdims=True)
        sums = jnp.where(lane == 2 * p, lower, jnp.where(lane == 2 * p + 1, upper, sums))
    small[:groups, :] = sums.T[:groups]
    for p in range(pairs):
        cut = pl.ds(p * lanes, lanes)
        small[groups + p:groups + p + 1, :] = gain_grad[:, cut]
        small[groups + pairs + p:groups + pairs + p + 1, :] = shift_grad[:, cut]
    small_swap = remote(small, small_in, core_sem.at[0, 1], core_sem.at[1, 1], partner)
    small_swap.start()
    copies = {}
    token_swap.wait()
    grad_swap.wait()

    def send_chunk(i):
        target = (z + 1 + i) % levels
        cut = pl.ds(pl.multiple_of(target * depth, depth), depth)
        product = lax.dot_general(
            tokens[:, cut], own_part[...], (((0,), (0,)), ((), ())), preferred_element_type=F32
        ) + lax.dot_general(
            peer_tokens[:, cut], peer_grads[...], (((0,), (0,)), ((), ())), preferred_element_type=F32
        )
        part[i] = product.reshape(part.shape[1:]).astype(BF16)
        for k in range(1, ways):
            copy = remote(
                part.at[i, :, (s + k) % ways], plane_in.at[i, k - 1],
                plane_sem.at[0, i, k - 1], plane_sem.at[1, i, k - 1], in_plane(k),
            )
            copy.start()
            copies[i, k] = copy

    send_chunk(0)
    mix_swap.wait()
    small_swap.wait()
    mix_low[...] = (mix_part[c] + mix_in[...]).astype(BF16)
    small_plane[s] = small[...] + small_in[...]
    mix_copies, small_copies = [], []
    for k in range(1, ways):
        mix_copies.append(remote(
            mix_low.at[(s + k) % ways], mix_plane.at[k - 1],
            mix_sem.at[0, k - 1], mix_sem.at[1, k - 1], in_plane(k),
        ))
        small_copies.append(remote(
            small_plane.at[s], small_plane.at[s],
            small_sem.at[0, k - 1], small_sem.at[1, k - 1], in_plane(k),
        ))
    for copy in mix_copies + small_copies:
        copy.start()
    for i in range(1, levels):
        send_chunk(i)
    for k in late:
        forward(k)
    for k in early:
        relay_all(k)
    project(weights[...], d)
    shard_swap.wait()
    project(gathered[z, 1 - c], z * CORES + 1 - c)

    mix_level_copies, small_level_copies, mix_up, mix_gather = [], [], [], []

    def mix_stage(stage):
        if stage == 0:
            for copy in mix_copies + small_copies:
                copy.wait()
            total = mix_low[s].astype(F32)
            for k in range(1, ways):
                total = total + mix_plane[k - 1].astype(F32)
            mix_sum[...] = total
            mix_level_out[...] = total.astype(BF16)
            gathered_small = small_plane[0]
            for k in range(1, ways):
                gathered_small = gathered_small + small_plane[k]
            small_level[z] = gathered_small
            for k in range(1, levels):
                mix_level_copies.append(remote(
                    mix_level_out.at[(z + k) % levels], mix_level.at[k - 1],
                    mix_level_sem.at[0, k - 1], mix_level_sem.at[1, k - 1], in_level(k),
                ))
                small_level_copies.append(remote(
                    small_level.at[z], small_level.at[z],
                    small_level_sem.at[0, k - 1], small_level_sem.at[1, k - 1], in_level(k),
                ))
            for copy in mix_level_copies + small_level_copies:
                copy.start()
        elif stage == 1:
            for copy in mix_level_copies + small_level_copies:
                copy.wait()
            total = mix_sum[z]
            for k in range(1, levels):
                total = total + mix_level[k - 1].astype(F32)
            mix_out[c, s, z] = total.astype(BF16)
            gathered_small = small_level[0]
            for k in range(1, levels):
                gathered_small = gathered_small + small_level[k]
            small_out[...] = gathered_small
            for k in range(1, levels):
                block = mix_out.at[c, s, z]
                mix_up.append(remote(
                    block, block, mix_up_sem.at[0, k - 1], mix_up_sem.at[1, k - 1], in_level(k)
                ))
                mix_up[-1].start()
        else:
            for copy in mix_up:
                copy.wait()
            for k in range(1, ways):
                block = mix_out.at[c, s]
                mix_gather.append(remote(
                    block, block, mix_out_sem.at[0, k - 1], mix_out_sem.at[1, k - 1], in_plane(k)
                ))
                mix_gather[-1].start()

    stages = [0, 1, 2]
    level_copies = []
    for i in range(levels):
        total = part[i, :, s].astype(F32)
        for k in range(1, ways):
            copies[i, k].wait_recv()
            total = total + plane_in[i, k - 1].astype(F32)
        if i < levels - 1:
            level_out[i] = total.astype(BF16)
            copy = remote(
                level_out.at[i], level_in.at[i], level_sem.at[0, i], level_sem.at[1, i], in_level(i + 1)
            )
            copy.start()
            level_copies.append(copy)
            if stages:
                mix_stage(stages.pop(0))
            if i < len(early):
                project_level(early[i])
        else:
            own_sum[...] = total
    total = own_sum[...]
    for i in range(levels - 1):
        level_copies[i].wait_recv()
        total = total + level_in[i].astype(F32)
    final[...] = total
    final_swap = remote(final.at[1 - c], final_in, core_sem.at[0, 2], core_sem.at[1, 2], partner)
    final_swap.start()
    while stages:
        mix_stage(stages.pop(0))
    final_swap.wait()
    mine, theirs = final[c], final_in[...]
    lower_half = jnp.full(mine.shape, c, jnp.int32) == 0
    summed[s, :, :channels] = jnp.where(lower_half, mine, theirs).astype(BF16)
    summed[s, :, channels:] = jnp.where(lower_half, theirs, mine).astype(BF16)
    gather = []
    for k in range(1, ways):
        copy = remote(
            summed.at[s], summed.at[s], gather_sem.at[0, k - 1], gather_sem.at[1, k - 1], in_plane(k)
        )
        copy.start()
        gather.append(copy)
    for k in late:
        relay_all(k)
    for k in late:
        project_level(k)
    for copy in mix_gather:
        copy.wait()
    mix_back = remote(mix_out.at[c], mix_out.at[c], core_sem.at[0, 3], core_sem.at[1, 3], partner)
    mix_back.start()
    mix_back.wait()
    for copy in gather:
        copy.wait()
    for copy in level_copies + shard_copies:
        copy.wait_send()
    for pile in (copies, spreads, relays):
        for key in pile:
            pile[key].wait_send()


def shards(
    tokens,
    value_act,
    gate_act,
    cotangent,
    value_weight,
    gate_weight,
    norm_gain,
    norm_bias,
    mix_weight,
    mix_bias,
):
    ways = lax.axis_size("sp")
    levels = lax.axis_size("dp") // CORES
    inputs = tokens[0]
    seq_len, width = inputs.shape
    channels = value_act.shape[2]
    groups, block_len = mix_weight.shape[0], mix_weight.shape[1]
    group_dim = channels // groups
    pairs = groups // 2
    lanes = channels // pairs
    rows = value_weight.shape[0]
    share = rows // ways
    vmem = pl.BlockSpec(memory_space=pltpu.VMEM)
    sems = pltpu.SemaphoreType.DMA
    weights = jnp.concatenate((value_weight, gate_weight), axis=1)
    causal = jnp.tril(jnp.ones((block_len, block_len), dtype=bool))
    masked = jnp.where(causal[None], mix_weight, jnp.zeros_like(mix_weight))
    mix = masked.reshape(pairs, 2 * block_len, block_len)
    bias = jnp.repeat(mix_bias.T, group_dim, axis=1)
    low_rows = groups * block_len // (CORES * ways * levels)
    mix_shape = (CORES, ways, levels, low_rows, block_len)
    small_shape = (groups + 2 * pairs, lanes)
    shape = jax.ShapeDtypeStruct
    input_grad, summed, mix_out, small_out = pl.pallas_call(
        functools.partial(kernel, ways, levels),
        out_shape=(
            shape((seq_len, width), BF16),
            shape((ways, share, 2 * channels), BF16),
            shape(mix_shape, BF16),
            shape(small_shape, F32),
        ),
        in_specs=[vmem] * 10,
        out_specs=(vmem,) * 4,
        scratch_shapes=[
            pltpu.VMEM((seq_len, 2 * channels), BF16),
            pltpu.VMEM((seq_len, width), BF16),
            pltpu.VMEM((seq_len, channels), BF16),
            pltpu.VMEM((levels, CORES, rows, 2 * channels), BF16),
            pltpu.VMEM((pairs, 2 * block_len, block_len), F32),
            pltpu.VMEM((block_len, channels), F32),
            pltpu.VMEM((1, channels), F32),
            pltpu.VMEM((1, channels), F32),
            pltpu.VMEM((seq_len, channels), BF16),
            pltpu.VMEM((seq_len, channels), BF16),
            pltpu.VMEM((block_len, channels), BF16),
            pltpu.VMEM((block_len, channels), BF16),
            pltpu.VMEM((block_len, channels), F32),
            pltpu.VMEM((block_len, channels), F32),
            pltpu.VMEM((levels, CORES, ways, share, channels), BF16),
            pltpu.VMEM(mix_shape, F32),
            pltpu.VMEM(small_shape, F32),
            pltpu.VMEM((levels, ways - 1, CORES, share, channels), BF16),
            pltpu.VMEM((levels - 1, CORES, share, channels), BF16),
            pltpu.VMEM((levels - 1, CORES, share, channels), BF16),
            pltpu.VMEM((CORES, share, channels), F32),
            pltpu.VMEM((CORES, share, channels), F32),
            pltpu.VMEM((share, channels), F32),
            pltpu.VMEM(mix_shape[1:], F32),
            pltpu.VMEM(mix_shape[1:], BF16),
            pltpu.VMEM((ways - 1,) + mix_shape[2:], BF16),
            pltpu.VMEM(mix_shape[2:], F32),
            pltpu.VMEM(mix_shape[2:], BF16),
            pltpu.VMEM((levels - 1,) + mix_shape[3:], BF16),
            pltpu.VMEM(small_shape, F32),
            pltpu.VMEM((ways,) + small_shape, F32),
            pltpu.VMEM((levels,) + small_shape, F32),
            sems((2, 3)),
            sems((2, levels - 1)),
            sems((2, levels - 1, ways - 1)),
            sems((2, levels - 1, ways)),
            sems((2, 4)),
            sems((2, levels, ways - 1)),
            sems((2, levels - 1)),
            sems((2, ways - 1)),
            sems((2, ways - 1)),
            sems((2, levels - 1)),
            sems((2, levels - 1)),
            sems((2, ways - 1)),
            sems((2, ways - 1)),
            sems((2, levels - 1)),
        ],
        compiler_params=pltpu.CompilerParams(
            collective_id=0, has_side_effects=True, vmem_limit_bytes=60 * 1024 * 1024
        ),
        name="unit",
    )(
        inputs, weights, value_act[0], gate_act[0], cotangent[0],
        norm_gain[None], norm_bias[None], mix, mix.transpose(0, 2, 1), bias,
    )
    weight_sums = summed.reshape(rows, 2 * channels).astype(F32)
    mix_grad = jnp.where(causal[None], mix_out.reshape(groups, block_len, block_len).astype(F32), 0.0)
    small_out = small_out.reshape(-1)
    biases = groups * block_len
    return (
        input_grad[None],
        weight_sums[:, :channels],
        weight_sums[:, channels:],
        mix_grad,
        small_out[:biases].reshape(groups, block_len),
        small_out[biases:biases + channels],
        small_out[biases + channels:],
    )


def solution(mesh):
    placed = (
        P("dp", "sp", None),
        P("dp", "sp", None),
        P("dp", "sp", None),
        P("dp", "sp", None),
        P("dp", None),
        P("dp", None),
        P(),
        P(),
        P(),
        P(),
    )
    return jax.shard_map(
        shards,
        mesh=mesh,
        in_specs=placed,
        out_specs=(P("dp", "sp", None), P("dp", None), P("dp", None), P(), P(), P(), P()),
        check_vma=False,
    )
```

time: 155 us -> 128 us (0.83)
  matrix products: 17.3 us -> 0 us
  Pallas kernels: 122 us -> 116 us
  local copies, waits for them, and re-layouts: 11.2 us -> 5.86 us
    dot_general x2 -> x0, matrix products: 17.3 us -> none  [the longest x1 10.2 us: shards(): lax.dot_general(both, gathered.reshape(width, 2 * channels), (((1,), (1,)...]
    pallas_call x2 -> x1, Pallas kernels: 122 us -> 116 us  [shards(): pl.pallas_call(functools.partial(kernel, ways, levels), out_shape=(shape(...]
    unnamed x28 -> x13, local copies, waits for them, and re-layouts: 6.1 us -> 1.17 us
where the time goes in v2:
time: 128 us
  Pallas kernels  116 us (91%)
  local copies, waits for them, and re-layouts  5.86 us (5%)
  other arithmetic  4.91 us (4%)
    pallas_call x1, Pallas kernels, shards(): pl.pallas_call(functools.partial(kernel, ways, levels), out_shape=(shape(...  116 us

profile of v2, /device:TPU:0, one launch (start us, length us, event | category | flops | bytes accessed | tf_op | source)
XLA Modules:
  0.0 127.7 jit_solution(10331184937582174717)
XLA Ops:
  0.6 0.0 copy-start.3
  0.6 0.0 copy-start.5
  0.7 2.3 %pad_maximum_fusion.weights = bf16[256,2048]{1,0:T(8,128)(2,1)} fusion(bf16[256,1024]{1,0:T(8,128)(2,1)} %param.15, bf16[256,1024]{1,0:T(8,128)(2,1)} %param.14), kind=kLoop, calls=%fused_computation | loop fusion | flops 2097152 | bytes 2097152 | tf_op jit(solution)/shard_map/concatenate | solution.py:391
  3.0 0.0 copy-done.3
  3.1 0.0 copy-start
  3.1 1.0 copy.19
  4.1 0.0 copy-done.5
  4.1 1.0 copy.20.bias
  5.1 0.0 copy-done
  5.1 116.2 %unit.1 = (bf16[384,2048]{1,0:T(8,128)(2,1)}, bf16[4,64,2048]{2,1,0:T(8,128)(2,1)}, bf16[2,4,4,64,128]{4,3,2,1,0:T(8,128)(2,1)}, f32[32,128]{1,0:T(8,128)}) custom-call(bf16[384,2048]{1,0:T(8,128)(2,1)} %bitcast.25, bf16[256,2048]{1,0:T(8,128)(2,1)} %pad_maximum_fusion.weights, bf16[384,1024]{1,0:T(8,128)(2,1)} %bitcast.26, bf16[384,1024]{1,0:T(8,128)(2,1)} %bitcast.27, ...), custom_call_target="tpu_custom_call" | custom-call | tf_op jit(solution)/shard_map/unit/pallas_call | solution.py:400
  121.3 1.5 %bitcast_convert_fusion = f32[256,2048]{1,0:T(8,128)S(1)} fusion(bf16[4,64,2048]{2,1,0:T(8,128)(2,1)} %get-tuple-element.12), kind=kLoop, calls=%fused_computation.2 | loop fusion | flops 524288 | bytes 3145728 | tf_op jit(solution)/shard_map/convert_element_type | solution.py:466
  122.7 0.0 copy-start.2
  122.7 0.0 copy-start.4
  122.8 0.0 copy-start.1
  122.8 1.5 %fusion = (f32[256,1024]{1,0:T(8,128)}, f32[256,1024]{1,0:T(8,128)}) fusion(f32[256,2048]{1,0:T(8,128)S(1)} %bitcast_convert_fusion), kind=kLoop, calls=%fused_computation.7 | loop fusion | bytes 4194304 | tf_op jit(solution)/shard_map/slice | solution.py:473
  124.2 0.0 copy-done.2
  124.2 1.1 convert_select_fusion
  125.3 0.0 copy-done.4
  125.3 0.6 slice.24
  125.9 0.6 slice_bitcast_fusion
  126.5 0.0 copy-done.1
  126.5 1.1 copy.22
  (3 shorter events, 0.1 us)
Async XLA Ops:
  0.6 2.4 %copy-start.3 = (bf16[16,128,128]{2,1,0:T(8,128)(2,1)S(1)}, bf16[16,128,128]{2,1,0:T(8,128)(2,1)}, u32[]{:S(2)}) copy-start(bf16[16,128,128]{2,1,0:T(8,128)(2,1)} %param.18) | copy-start | bytes 1572868
  0.6 3.4 %copy-start.5 = (f32[16,128]{1,0:T(8,128)S(1)}, f32[16,128]{1,0:T(8,128)}, u32[]{:S(2)}) copy-start(f32[16,128]{1,0:T(8,128)} %param.19) | copy-start | bytes 24580
  3.1 2.1 %copy-start = (bf16[16,128,128]{2,1,0:T(8,128)(2,1)}, bf16[16,128,128]{2,1,0:T(8,128)(2,1)S(1)}, u32[]{:S(2)}) copy-start(bf16[16,128,128]{2,1,0:T(8,128)(2,1)S(1)} %broadcast_select_fusion) | copy-start | bytes 1572868
  122.7 1.5 %copy-start.2 = (bf16[2,4,4,64,128]{4,3,2,1,0:T(8,128)(2,1)S(1)}, bf16[2,4,4,64,128]{4,3,2,1,0:T(8,128)(2,1)}, u32[]{:S(2)}) copy-start(bf16[2,4,4,64,128]{4,3,2,1,0:T(8,128)(2,1)} %get-tuple-element.13) | copy-start | bytes 1572868
  122.7 2.6 %copy-start.4 = (f32[32,128]{1,0:T(8,128)S(1)}, f32[32,128]{1,0:T(8,128)}, u32[]{:S(2)}) copy-start(f32[32,128]{1,0:T(8,128)} %get-tuple-element.14) | copy-start | bytes 49156
  122.8 3.7 %copy-start.1 = (bf16[384,2048]{1,0:T(8,128)(2,1)S(1)}, bf16[384,2048]{1,0:T(8,128)(2,1)}, u32[]{:S(2)}) copy-start(bf16[384,2048]{1,0:T(8,128)(2,1)} %get-tuple-element.11) | copy-start | bytes 4718596
